TPU v7x, 32 devices: a whole 2x2x4 slice. The times are simulated.
32 devices in a mesh: grp: 2 (over y), sp: 4 (over z), tp: 4 (over x, core).
Axes of the slice: x: 2, y: 2, z: 4, core: 2. Of those that a mesh axis runs over, the one named last changes fastest.
Arguments:
- query_rows: bfloat16 [1024, 1024], P(('grp', 'sp'), 'tp'), parts along dimension 0, may hold values from -12 to 12
- key_rows: bfloat16 [1024, 1024], P(('grp', 'sp'), 'tp'), parts along dimension 0, may hold values from -9 to 9
- value_rows: bfloat16 [1024, 1024], P(('grp', 'sp'), 'tp'), parts along dimension 0, may hold values from -6 to 6
- key_logit: bfloat16 [1024, 8], P(('grp', 'sp'), 'tp'), parts along dimension 0, as said below
- residual: bfloat16 [1024, 2048], P(('grp', 'sp')), parts along dimension 0, may hold values from -6 to 6
- out_weight: bfloat16 [1024, 2048], P('tp'), may hold values from -0.1875 to 0.1875
- mix_gain: float32 [2048], replicated, may hold values from 0.1 to 1.9
- ffn_gain: float32 [2048], replicated, may hold values from 0.1 to 1.9
- out_gain: float32 [2048], replicated, may hold values from 0.1 to 1.9
- gate_weight: bfloat16 [2048, 5120], P('sp', 'tp'), may hold values from -0.125 to 0.125
- up_weight: bfloat16 [2048, 5120], P('sp', 'tp'), may hold values from -0.125 to 0.125
- down_weight: bfloat16 [2048, 5120], P('sp', 'tp'), may hold values from -0.078125 to 0.078125
Outputs:
- layer_out: bfloat16 [1024, 2048], P(('grp', 'sp')), parts along dimension 0
There are 2 independent parts, one for each index of `grp`. A program takes and returns all parts, laid end to end along the dimension named above; an argument that names none is the same for every part. Nothing has to cross between parts.
Inputs may be any that keep to these rules, and one draw needn't show every extreme that they name: `key_logit`: log-odds offsets of the keys, all negative.
All inputs are finite; a program needn't handle non-finite values.
Results may differ from a plain program's by a relative error of at most 0.018.
Values may be sent and summed in bfloat16 or wider, within the bound.
A program may use at most 64 MiB of HBM per device.

v0:
```python
import jax
import jax.numpy as jnp
from jax import lax
from jax.sharding import PartitionSpec as P

epsilon = 1e-06


def normalize(payload_table):
    return payload_table * lax.rsqrt(
        jnp.mean(payload_table * payload_table, axis=-1, keepdims=True) + epsilon
    )


def shards(
    query_rows,
    key_rows,
    value_rows,
    key_logit,
    residual,
    out_weight,
    mix_gain,
    ffn_gain,
    out_gain,
    gate_weight,
    up_weight,
    down_weight,
):
    tok_rows = query_rows.shape[0]
    head_count = key_logit.shape[1]
    head_width = query_rows.shape[1] // head_count
    block_count = lax.axis_size("sp")
    own_block = lax.axis_index("sp")
    queries = query_rows.reshape(tok_rows, head_count, head_width).transpose(1, 0, 2)
    score_scale = head_width ** (-0.5)
    query_pos = own_block * tok_rows + jnp.arange(tok_rows, dtype=jnp.int32)[:, None]

    def group_terms(key_part, value_part, logit_part, first_block):
        span_rows = key_part.shape[0]
        shard_count = span_rows // tok_rows

        def compute(unused):
            scores = (
                jnp.einsum(
                    "hqd,khd->hqk",
                    queries,
                    key_part.reshape(span_rows, head_count, head_width),
                    preferred_element_type=jnp.float32,
                )
                * score_scale
            )
            scores = scores + jnp.transpose(logit_part.astype(jnp.float32))[:, None, :]
            key_pos = first_block * tok_rows + jnp.arange(span_rows, dtype=jnp.int32)[None, :]
            causal = (key_pos < query_pos).reshape(tok_rows, shard_count, tok_rows)
            scores = scores.reshape(head_count, tok_rows, shard_count, tok_rows)
            keep_log = jnp.where(causal, jax.nn.log_sigmoid(-scores), 0.0)
            within = lax.cumsum(keep_log, axis=3, reverse=True) - keep_log
            sticks = jnp.where(causal, jnp.exp(jax.nn.log_sigmoid(scores) + within), 0.0).astype(
                jnp.bfloat16
            )
            partials = jnp.einsum(
                "hqgk,gkhd->ghqd",
                sticks,
                value_part.reshape(shard_count, tok_rows, head_count, head_width),
                preferred_element_type=jnp.float32,
            )
            return (jnp.sum(keep_log, axis=3), partials)

        def skipped(unused):
            return (
                jnp.zeros((head_count, tok_rows, shard_count), jnp.float32),
                jnp.zeros((shard_count, head_count, tok_rows, head_width), jnp.float32),
            )

        return lax.cond(first_block <= own_block, compute, skipped, 0)

    initial = (
        jnp.zeros((head_count, tok_rows, block_count), jnp.float32),
        jnp.zeros((block_count, head_count, tok_rows, head_width), jnp.float32),
    )
    tables = initial
    key_part = lax.all_gather(key_rows, "sp", axis=0, tiled=True)
    value_part = lax.all_gather(value_rows, "sp", axis=0, tiled=True)
    logit_part = lax.all_gather(key_logit, "sp", axis=0, tiled=True)
    shard_count = key_part.shape[0] // tok_rows
    group_size = 2
    span_rows = group_size * tok_rows

    def one_group(carried, group_index):
        offset = group_index * span_rows
        first_block = group_index * group_size
        totals, partials = group_terms(
            lax.dynamic_slice_in_dim(key_part, offset, span_rows, 0),
            lax.dynamic_slice_in_dim(value_part, offset, span_rows, 0),
            lax.dynamic_slice_in_dim(logit_part, offset, span_rows, 0),
            first_block,
        )
        carried = (
            lax.dynamic_update_slice(carried[0], totals, (0, 0, first_block)),
            lax.dynamic_update_slice(carried[1], partials, (first_block, 0, 0, 0)),
        )
        return (carried, None)

    tables, unused = lax.scan(
        one_group, tables, jnp.arange(shard_count // group_size, dtype=jnp.int32)
    )
    totals, partials = tables
    suffix = lax.cumsum(totals, axis=2, reverse=True) - totals
    attended = jnp.einsum(
        "hqb,bhqd->qhd", jnp.exp(suffix), partials, precision=lax.Precision.HIGHEST
    )
    attended = attended.reshape(tok_rows, head_count * head_width).astype(jnp.bfloat16)
    head_part = jnp.dot(attended, out_weight, preferred_element_type=jnp.float32)
    mixed_rows = lax.psum(head_part.astype(jnp.bfloat16), "tp")
    middle = (
        residual.astype(jnp.float32) + mix_gain * normalize(mixed_rows.astype(jnp.float32))
    ).astype(jnp.bfloat16)
    normed = (ffn_gain * normalize(middle.astype(jnp.float32))).astype(jnp.bfloat16)
    gate_act = jnp.dot(
        normed,
        lax.all_gather(gate_weight, "sp", axis=0, tiled=True),
        preferred_element_type=jnp.float32,
    )
    up_act = jnp.dot(
        normed,
        lax.all_gather(up_weight, "sp", axis=0, tiled=True),
        preferred_element_type=jnp.float32,
    )
    hidden = (jax.nn.silu(gate_act) * up_act).astype(jnp.bfloat16)
    unit_part = lax.dot_general(
        hidden,
        lax.all_gather(down_weight, "sp", axis=0, tiled=True),
        (((1,), (1,)), ((), ())),
        preferred_element_type=jnp.float32,
    )
    ffn_out = lax.psum(unit_part.astype(jnp.bfloat16), "tp")
    return (middle.astype(jnp.float32) + out_gain * normalize(ffn_out.astype(jnp.float32))).astype(
        jnp.bfloat16
    )


def solution(mesh):
    placed = (
        P(("grp", "sp"), "tp"),
        P(("grp", "sp"), "tp"),
        P(("grp", "sp"), "tp"),
        P(("grp", "sp"), "tp"),
        P(("grp", "sp"), None),
        P("tp", None),
        P(),
        P(),
        P(),
        P("sp", "tp"),
        P("sp", "tp"),
        P("sp", "tp"),
    )
    return jax.shard_map(
        shards, mesh=mesh, in_specs=placed, out_specs=P(("grp", "sp"), None), check_vma=False
    )
```

profile of v0, /device:TPU:1, one launch (start us, length us, event | category | flops | bytes accessed | tf_op | source)
XLA Modules:
  0.0 406.7 jit_solution(9131922966451456633)
XLA Ops:
  7.4 0.0 copy-start
  7.4 0.0 all-reduce.3.cloned.1.call-start
  7.4 1.0 copy.41
  8.4 12.4 %all_gather.18 = bf16[512,256]{0,1:T(8,128)(2,1)S(1)} all-gather(bf16[128,256]{0,1:T(8,128)(2,1)S(1)} %copy.41), channel_id=1, replica_groups=mesh['grp'=2,'sp'=4,'tp'=4] {'sp'}, dimensions={0}, use_global_device_ids=true | all-gather | bytes 327680 | tf_op jit(solution)/shard_map/all_gather | solution.py:82
  20.8 11.1 %all_gather.20 = bf16[512,256]{1,0:T(8,128)(2,1)S(1)} all-gather(bf16[128,256]{1,0:T(8,128)(2,1)} %param.18), channel_id=1, replica_groups=mesh['grp'=2,'sp'=4,'tp'=4] {'sp'}, dimensions={0}, use_global_device_ids=true | all-gather | bytes 327680 | tf_op jit(solution)/shard_map/all_gather | solution.py:83
  31.9 0.9 copy.42
  32.9 0.1 copy.43
  33.0 8.3 %all_gather.19 = bf16[512,2]{0,1:T(2,128)(2,1)S(1)} all-gather(bf16[128,2]{0,1:T(2,128)(2,1)} %param.19), channel_id=1, replica_groups=mesh['grp'=2,'sp'=4,'tp'=4] {'sp'}, dimensions={0}, use_global_device_ids=true | all-gather | bytes 2560 | tf_op jit(solution)/shard_map/all_gather | solution.py:84
  41.3 0.1 broadcast_in_dim.28.clone
  41.4 8.5 %while.13 = (s32[]{:T(128)}, f32[2,128,4]{1,2,0:T(4,128)S(1)}, f32[4,2,128,128]{3,0,1,2:T(4,128)S(1)}, s32[2]{0:T(128)S(1)}, s32[]{:T(128)}, /*index=5*/bf16[512...) while((s32[]{:T(128)}, f32[2,128,4]{1,2,0:T(4,128)S(1)}, ...), condition=%wide.region_5.6_spmd.clone, body=%wide.region_0.5_spmd.clone.sunk | while | flops 43418504 | bytes 4373875 | solution.py:104
  41.4 0.6 dynamic_slice.39
  42.6 5.3 %conditional.3 = (f32[2,128,2]{1,2,0:T(2,128)S(1)}, f32[2,2,128,128]{3,2,1,0:T(8,128)S(1)}) conditional(s32[]{:T(128)} %convert_element_type.116, () %tuple.48, (s32[]{:T(128)}, s32[]{:T(128)}, s32[]{:T(128)}, bf16[512,256]{0,1:T(8,128)(2,1)S(1)}, bf16[2,128,128]{2,1,0:T(8,128)(2,1)S(1)}, /*index=5*/bf16[512,2]{0,1:T(2,128)(2,1)S(1)}, ...), branch_computations={%region_1.1_spmd, %region_2.4_spmd} | conditional | flops 43418500 | bytes 3844702 | solution.py:75
  43.3 0.2 fusion.2
  43.6 0.2 broadcast_compare_fusion
  43.8 0.8 fusion.35
  44.6 2.2 fusion.38
  46.7 0.9 select_convert_fusion
  47.7 0.2 fusion.8
  48.0 0.3 copy_dynamic-update-slice_fusion.2
  48.3 0.6 dynamic_slice.39
  49.6 0.3 copy_dynamic-update-slice_fusion.2
  49.9 0.0 copy-start.1
  49.9 0.0 copy-start.2
  50.0 0.0 copy-start.3
  50.0 0.2 copy.45
  50.2 1.8 fusion.39
  52.0 0.0 copy-done
  52.0 1.1 convolution_convert_fusion.1
  53.1 0.0 all-reduce.3.cloned.1.call-update
  53.2 0.0 all-gather.4.cloned.1.call-start
  53.2 0.5 all-gather.4.cloned.1.call-update
  53.7 0.0 all-gather.6.cloned.1.call-start
  53.8 0.5 all-gather.6.cloned.1.call-update
  54.3 0.0 all-gather.8.cloned.1.call-start
  54.4 0.5 all-gather.8.cloned.1.call-update
  54.9 0.0 all-reduce.5.cloned.1.call-start
  55.0 39.8 %all-reduce.3.cloned.1.call-done = bf16[128,2048]{1,0:T(8,128)(2,1)} async-done(((bf16[128,2048]{1,0:T(8,128)(2,1)}), bf16[128,2048]{1,0:T(8,128)(2,1)}) %all-reduce.3.cloned.1.call-update) | async-done | bytes 524304 | tf_op jit(solution)/shard_map/psum | solution.py:114
  94.7 1.2 fusion.12
  96.0 0.0 copy-done.1
  96.0 0.0 copy-done.2
  96.0 1.5 fusion.18
  97.4 65.0 %all-gather.4.cloned.1.call-done = bf16[2048,1280]{1,0:T(8,128)(2,1)} async-done(((bf16[512,1280]{1,0:T(8,128)(2,1)}), bf16[2048,1280]{1,0:T(8,128)(2,1)}) %all-gather.4.cloned.1.call-update) | async-done | bytes 5242896 | tf_op jit(solution)/shard_map/all_gather | solution.py:121
  162.4 0.0 copy-done.3
  162.4 3.4 fusion.30
  165.8 0.0 copy-start.4
  165.8 94.3 %all-gather.6.cloned.1.call-done = bf16[2048,1280]{1,0:T(8,128)(2,1)} async-done(((bf16[512,1280]{1,0:T(8,128)(2,1)}), bf16[2048,1280]{1,0:T(8,128)(2,1)}) %all-gather.6.cloned.1.call-update) | async-done | bytes 5242896 | tf_op jit(solution)/shard_map/all_gather | solution.py:126
  260.1 97.7 %all-gather.8.cloned.1.call-done = bf16[2048,1280]{1,0:T(8,128)(2,1)} async-done(((bf16[512,1280]{1,0:T(8,128)(2,1)}), bf16[2048,1280]{1,0:T(8,128)(2,1)}) %all-gather.8.cloned.1.call-update) | async-done | bytes 5242896 | tf_op jit(solution)/shard_map/all_gather | solution.py:132
  357.8 7.2 %convolution_convert_fusion = bf16[128,2048]{1,0:T(8,128)(2,1)} fusion(bf16[2048,1280]{1,0:T(8,128)(2,1)} %all-gather.8.cloned.1.call-done, bf16[2048,1280]{1,0:T(8,128)(2,1)} %all-gather.6.cloned.1.call-done, f32[128,1280]{1,0:T(8,128)S(1)} %fusion.30, bf16[128,2048]{1,0:T(8,128)(2,1)S(1)} %get-tuple-element.241, f32[128]{0:T(128)S(1)} %add_rsqrt_fusion.1, ...), kind=kOutput, calls=%fused_computation.23 | convolution fusion | flops 1344471040 | bytes 12198400 | tf_op jit(solution)/shard_map/dot_general | solution.py:130
  365.1 0.0 all-reduce.5.cloned.1.call-update
  365.1 30.7 %all-reduce.5.cloned.1.call-done = bf16[128,2048]{1,0:T(8,128)(2,1)} async-done(((bf16[128,2048]{1,0:T(8,128)(2,1)}), bf16[128,2048]{1,0:T(8,128)(2,1)}) %all-reduce.5.cloned.1.call-update) | async-done | bytes 524304 | tf_op jit(solution)/shard_map/psum | solution.py:136
  395.8 1.2 fusion.16
  397.0 0.0 copy-done.4
  397.0 2.1 fusion.21
  (21 shorter events, 0.3 us)
Async XLA Ops:
  7.4 44.7 %copy-start = (bf16[256,2048]{1,0:T(8,128)(2,1)S(1)}, bf16[256,2048]{1,0:T(8,128)(2,1)}, u32[]{:S(2)}) copy-start(bf16[256,2048]{1,0:T(8,128)(2,1)} %param.21) | copy-start | bytes 3145732
  7.4 87.4 %all-reduce.3.cloned.1.call-start = ((), (), s32[]{:S(2)}) async-start(), calls=%async_computation | async-start | bytes 1048576 | tf_op jit(solution)/shard_map/psum | solution.py:114
  49.9 46.0 %copy-start.1 = (bf16[128,2048]{1,0:T(8,128)(2,1)S(1)}, bf16[128,2048]{1,0:T(8,128)(2,1)}, u32[]{:S(2)}) copy-start(bf16[128,2048]{1,0:T(8,128)(2,1)} %param.20) | copy-start | bytes 1572868
  49.9 46.0 %copy-start.2 = (f32[2048]{0:T(1024)S(1)}, f32[2048]{0:T(1024)}, u32[]{:S(2)}) copy-start(f32[2048]{0:T(1024)} %param.22) | copy-start | bytes 24580
  50.0 112.5 %copy-start.3 = (f32[2048]{0:T(1024)S(1)}, f32[2048]{0:T(1024)}, u32[]{:S(2)}) copy-start(f32[2048]{0:T(1024)} %param.23) | copy-start | bytes 24580
  53.2 109.3 %all-gather.4.cloned.1.call-start = ((), (), s32[]{:S(2)}) async-start(), calls=%async_computation.1 | async-start | bytes 6553600 | tf_op jit(solution)/shard_map/all_gather | solution.py:121
  53.7 206.4 %all-gather.6.cloned.1.call-start = ((), (), s32[]{:S(2)}) async-start(), calls=%async_computation.2 | async-start | bytes 6553600 | tf_op jit(solution)/shard_map/all_gather | solution.py:126
  54.3 303.5 %all-gather.8.cloned.1.call-start = ((), (), s32[]{:S(2)}) async-start(), calls=%async_computation.3 | async-start | bytes 6553600 | tf_op jit(solution)/shard_map/all_gather | solution.py:132
  54.9 340.9 %all-reduce.5.cloned.1.call-start = ((), (), s32[]{:S(2)}) async-start(), calls=%async_computation.4 | async-start | bytes 1048576 | tf_op jit(solution)/shard_map/psum | solution.py:136
  165.8 231.2 %copy-start.4 = (f32[2048]{0:T(1024)S(1)}, f32[2048]{0:T(1024)}, u32[]{:S(2)}) copy-start(f32[2048]{0:T(1024)} %param.24) | copy-start | bytes 24580
Sparse Core Ops, SparseCore 0:
  53.3 41.4 all-reduce.2
  365.2 30.5 all-reduce.4
Sparse Core Ops, SparseCore 1:
  55.2 107.2 all-gather.3
  163.9 96.2 all-gather.5
  261.6 96.2 all-gather.7
where the time goes:
time: 409 us; the launch traced here: 407 us
  waiting for transfers between devices  329 us (80%)
  blocking collectives  31.8 us (8%)
  between operations  15.2 us (4%)
  matrix products  14 us (3%)
  other arithmetic  10.2 us (2%)
  local copies, waits for them, and re-layouts  4.28 us (1%)
    all_gather x1, waiting for transfers between devices, shards(): lax.all_gather(down_weight, 'sp', axis=0, tiled=True)  97.7 us
    all_gather x1, waiting for transfers between devices, shards(): lax.all_gather(up_weight, 'sp', axis=0, tiled=True)  94.3 us
    all_gather x1, waiting for transfers between devices, shards(): lax.all_gather(gate_weight, 'sp', axis=0, tiled=True)  65 us
    psum x1, waiting for transfers between devices, shards(): mixed_rows = lax.psum(head_part.astype(jnp.bfloat16), 'tp')  39.8 us
    psum x1, waiting for transfers between devices, shards(): ffn_out = lax.psum(unit_part.astype(jnp.bfloat16), 'tp')  30.7 us
    all_gather x1, blocking collectives, shards(): key_part = lax.all_gather(key_rows, 'sp', axis=0, tiled=True)  12.4 us
    all_gather x1, blocking collectives, shards(): value_part = lax.all_gather(value_rows, 'sp', axis=0, tiled=True)  11.1 us
    all_gather x1, blocking collectives, shards(): logit_part = lax.all_gather(key_logit, 'sp', axis=0, tiled=True)  8.31 us
  transfers between devices with their start and end apart: 5, of which 5 were waited for; matrix products, arithmetic and copies ran while one was open for 1% of the time, Pallas kernels for 0%

commit v1 on v0

v1 whole, which is shorter than its diff:
```python
import functools

import jax
import jax.numpy as jnp
from jax import lax
from jax.experimental import pallas as pl
from jax.experimental.pallas import tpu as pltpu
from jax.sharding import PartitionSpec as P

epsilon = 1e-06
MESH = pl.DeviceIdType.MESH
F32 = jnp.float32
BF16 = jnp.bfloat16


def normalize(rows):
    return rows * lax.rsqrt(jnp.mean(rows * rows, axis=-1, keepdims=True) + epsilon)


def each(count, body):
    if count <= 4:
        for i in range(count):
            body(i)
    else:

        def step(i, carry):
            body(i)
            return carry

        lax.fori_loop(0, count, step, 0)


def remote(src, dst, send, recv, axis, peer):
    return pltpu.make_async_remote_copy(
        src_ref=src,
        dst_ref=dst,
        send_sem=send,
        recv_sem=recv,
        device_id={axis: peer},
        device_id_type=MESH,
    )


def nt(a, b):
    return lax.dot_general(a, b, (((1,), (1,)), ((), ())), preferred_element_type=F32)


def kernel(
    S, TP, H,
    q, k, v, lg, mg, fg, og, res, ow, gw, uw, dw,
    out,
    kb, vb, lb, acc, run, owv, gwv, uwv, dwv, resv,
    hs, hr, mid, ns, na, tmp, gs, gr, hall, us, ur, zs, zr, oall,
    loc, kvs, kvr, hss, hrs, n1s, n1r, n2s, n2r, gss, grs, hars, hals, har,
    upss, upr, zss, zrs, oss, ors, outs,
):
    me, tp = lax.axis_index("sp"), lax.axis_index("tp")
    T = q.shape[0]
    hd = q.shape[1] // H
    D = out.shape[1]
    R, C = T // TP, D // S
    right, left = lax.rem(me + 1, S), lax.rem(me + S - 1, S)

    my_rows = pl.ds(pl.multiple_of(tp * R, R), R)
    loads = [
        pltpu.make_async_copy(a, b, loc.at[i])
        for i, (a, b) in enumerate(
            [(ow, owv), (res.at[my_rows], resv), (gw, gwv), (uw, uwv), (dw, dwv)]
        )
    ]
    for c in loads:
        c.start()

    barrier = pltpu.get_barrier_semaphore()
    for f in range(1, S):
        pl.semaphore_signal(barrier, inc=1, device_id={"sp": lax.rem(me + f, S)}, device_id_type=MESH)
    for f in range(1, TP):
        pl.semaphore_signal(barrier, inc=1, device_id={"tp": lax.rem(tp + f, TP)}, device_id_type=MESH)
    pl.semaphore_wait(barrier, S + TP - 2)

    def kv_copies(b, own):
        srcs = (k, v, lg) if own else (kb.at[b], vb.at[b], lb.at[b])
        return [
            remote(src, dst.at[b], kvs.at[b, i], kvr.at[b, i], "sp", right)
            for i, (src, dst) in enumerate(zip(srcs, (kb, vb, lb)))
        ]

    @pl.when(me < S - 1)
    def _():
        for c in kv_copies(me, True):
            c.start()

    rows = lax.broadcasted_iota(jnp.int32, (T, T), 0)
    cols = lax.broadcasted_iota(jnp.int32, (T, T), 1)
    causal = cols < rows
    later = (rows > cols).astype(F32)

    def block(kk, vv, ll, diag):
        for h in range(H):
            span = slice(h * hd, (h + 1) * hd)
            s = nt(q[:, span], kk[:, span]) * (hd**-0.5) + ll[h : h + 1, :]
            soft = jnp.log1p(jnp.exp(-jnp.abs(s)))
            keep = jnp.minimum(-s, 0.0) - soft
            logsig = jnp.minimum(s, 0.0) - soft
            if diag:
                keep = jnp.where(causal, keep, 0.0)
            within = jnp.dot(
                keep, later, preferred_element_type=F32, precision=lax.Precision.HIGHEST
            )
            stick = jnp.exp(logsig + within)
            if diag:
                stick = jnp.where(causal, stick, 0.0)
            part = jnp.dot(stick.astype(BF16), vv[:, span], preferred_element_type=F32)
            total = jnp.broadcast_to(jnp.sum(keep, axis=-1, keepdims=True), (T, hd))
            if diag:
                acc[h] = part
                run[h] = total
            else:
                acc[h] += jnp.exp(run[h]) * part
                run[h] += total

    block(k[...], v[...], lg[...], True)

    def earlier(i):
        b = me - 1 - i

        @pl.when(b >= 0)
        def _():
            for c in kv_copies(b, False):
                c.wait_recv()

            @pl.when(me < S - 1)
            def _():
                for c in kv_copies(b, False):
                    c.start()

            block(kb[b], vb[b], lb[b], False)

    each(S - 1, earlier)

    attended = jnp.concatenate([acc[h] for h in range(H)], axis=1).astype(BF16)
    loads[0].wait()
    width = 512 if D % 512 == 0 else D
    for c0 in range(0, D, width):
        piece = jnp.dot(attended, owv[:, c0 : c0 + width], preferred_element_type=F32)
        hs[:, :, c0 : c0 + width] = piece.astype(BF16).reshape(TP, R, width)

    def hp_copy(t, slot):
        return remote(hs.at[t], hr.at[slot], hss.at[t], hrs.at[slot], "tp", t)

    def others(count, own, body):
        def go(i):
            body(lax.rem(own + 1 + i, count))

        each(count - 1, go)

    others(TP, tp, lambda t: hp_copy(t, tp).start())
    mid[...] = hs[tp].astype(F32)

    def add_hp(t):
        hp_copy(t, t).wait_recv()
        mid[...] += hr[t].astype(F32)

    others(TP, tp, add_hp)
    loads[1].wait()
    mixed = mid[...].astype(BF16).astype(F32)
    middle = (resv[...].astype(F32) + mg[...] * normalize(mixed)).astype(BF16).astype(F32)
    mid[...] = middle
    normed = (fg[...] * normalize(middle)).astype(BF16)
    for j in range(S):
        ns[j] = normed[:, j * C : (j + 1) * C]

    def n1_copy(j, slot):
        return remote(ns.at[j], na.at[tp, slot], n1s.at[j], n1r.at[slot], "sp", j)

    def n2_copy(t, slot, s):
        return remote(na.at[tp, s], na.at[slot, s], n2s.at[t, s], n2r.at[slot, s], "tp", t)

    others(S, me, lambda j: n1_copy(j, me).start())
    na[tp, me] = ns[me]
    others(TP, tp, lambda t: n2_copy(t, tp, me).start())

    def pass_on(s):
        n1_copy(s, s).wait_recv()
        others(TP, tp, lambda t: n2_copy(t, tp, s).start())

    others(S, me, pass_on)
    for c in loads[2:4]:
        c.wait()

    def arrive(s):
        others(TP, tp, lambda t: remote(na.at[tp, s], na.at[t, s], n2s.at[t, s], n2r.at[t, s], "tp", t).wait_recv())

    def partial(j):
        arrive(j)
        x = na[:, j].reshape(T, C)
        tmp[0] = jnp.dot(x, gwv[...], preferred_element_type=F32)
        tmp[1] = jnp.dot(x, uwv[...], preferred_element_type=F32)

    def g_copy(j, slot, i, peer):
        return remote(gs.at[j, i], gr.at[slot, i], gss.at[j, i], grs.at[slot, i], "sp", peer)

    def chain(j, first, slot, peer):
        partial(j)

        @pl.when(first)
        def _():
            for i in range(2):
                gs[j, i] = tmp[i].astype(BF16)
                g_copy(j, slot, i, peer).start()

        @pl.when(jnp.logical_not(first))
        def _():
            for i in range(2):
                g_copy(j, j, i, peer).wait_recv()
                gs[j, i] = (tmp[i] + gr[j, i].astype(F32)).astype(BF16)
                g_copy(j, slot, i, peer).start()

    def reduce_step(tau, carry):
        jr = S - 1 - tau + me
        jl = tau - (S - 1 - me)

        @pl.when((jr > me) & (jr < S))
        def _():
            chain(jr, me == 0, jr, right)

        @pl.when((jl >= 0) & (jl < me))
        def _():
            chain(jl, me == S - 1, lax.select(jl == me - 1, S, jl), left)

        return carry

    lax.fori_loop(0, S - 1, reduce_step, 0)
    partial(me)
    for i in range(2):

        @pl.when(me > 0)
        def _():
            g_copy(me, me, i, left).wait_recv()
            tmp[i] += gr[me, i].astype(F32)

        @pl.when(me < S - 1)
        def _():
            g_copy(me, S, i, right).wait_recv()
            tmp[i] += gr[S, i].astype(F32)

    gate = tmp[0]
    hall[me] = (gate / (1.0 + jnp.exp(-gate)) * tmp[1]).astype(BF16)

    def h_right(b):
        return remote(hall.at[b], hall.at[b], hars.at[b], har.at[b], "sp", right)

    def h_left(b):
        return remote(hall.at[b], hall.at[b], hals.at[b], har.at[b], "sp", left)

    @pl.when(me < S - 1)
    def _():
        h_right(me).start()

    @pl.when(me > 0)
    def _():
        h_left(me).start()

    def up_copy(t, slot, b):
        return remote(us.at[t, b], ur.at[slot, b], upss.at[t, b], upr.at[slot, b], "tp", t)

    def down(b):
        us[:, b] = nt(hall[b], dwv[...]).astype(BF16).reshape(TP, R, C)
        others(TP, tp, lambda t: up_copy(t, tp, b).start())

    def z_copy(b, slot):
        return remote(zs.at[b], zr.at[slot], zss.at[b], zrs.at[slot], "sp", b)

    def settle(b):
        total = us[tp, b].astype(F32)
        mid2 = [total]

        def add(t):
            up_copy(t, t, b).wait_recv()
            zs_sum[...] += ur[t, b].astype(F32)

        zs_sum = tmp.at[0, pl.ds(0, R), pl.ds(0, C)]
        zs_sum[...] = mid2[0]
        others(TP, tp, add)
        zs[b] = zs_sum[...].astype(BF16)

        @pl.when(b != me)
        def _():
            z_copy(b, me).start()

    loads[4].wait()
    down(me)

    def spread(i, carry):
        lo, hi = me - 1 - i, me + 1 + i

        @pl.when(lo >= 0)
        def _():
            h_right(lo).wait_recv()

            @pl.when(me < S - 1)
            def _():
                h_right(lo).start()

            down(lo)

        @pl.when(hi < S)
        def _():
            h_left(hi).wait_recv()

            @pl.when(me > 0)
            def _():
                h_left(hi).start()

            down(hi)

        return carry

    lax.fori_loop(0, S - 1, spread, 0)
    others(S, me, settle)
    settle(me)
    zr[me] = zs[me]
    others(S, me, lambda s: z_copy(s, s).wait_recv())
    ffn = jnp.concatenate([zr[s] for s in range(S)], axis=1).astype(F32)
    oall[tp] = (mid[...] + og[...] * normalize(ffn)).astype(BF16)

    def o_copy(t, slot):
        return remote(oall.at[tp], oall.at[slot], oss.at[t], ors.at[slot], "tp", t)

    def o_out(t):
        return pltpu.make_async_copy(
            oall.at[t], out.at[pl.ds(pl.multiple_of(t * R, R), R)], outs.at[t]
        )

    others(TP, tp, lambda t: o_copy(t, tp).start())
    o_out(tp).start()

    def o_in(t):
        remote(oall.at[tp], oall.at[t], oss.at[t], ors.at[t], "tp", t).wait_recv()
        o_out(t).start()

    others(TP, tp, o_in)
    each(TP, lambda t: o_out(t).wait())

    @pl.when(me < S - 1)
    def _():
        def sent(b):
            @pl.when(b <= me)
            def _():
                for c in kv_copies(b, False):
                    c.wait_send()
                h_right(b).wait_send()

        each(S, sent)

    @pl.when(me > 0)
    def _():
        def sent(b):
            @pl.when(b >= me)
            def _():
                h_left(b).wait_send()

        each(S, sent)

    def sp_sent(j):
        n1_copy(j, me).wait_send()
        z_copy(j, me).wait_send()
        for i in range(2):
            g_copy(j, j, i, right).wait_send()

    others(S, me, sp_sent)

    def tp_sent(t):
        hp_copy(t, tp).wait_send()
        o_copy(t, tp).wait_send()

        def inner(s):
            n2_copy(t, tp, s).wait_send()
            up_copy(t, tp, s).wait_send()

        each(S, inner)

    others(TP, tp, tp_sent)


def solution(mesh):
    S, TP = mesh.shape["sp"], mesh.shape["tp"]

    def shards(q, k, v, lg, res, ow, mg, fg, og, gw, uw, dw):
        T, H = lg.shape
        hw = q.shape[1]
        D = res.shape[1]
        C, U = gw.shape
        R = T // TP
        pad = -H % 8
        lgt = jnp.pad(lg.astype(F32).T, ((0, pad), (0, 0)))
        vm = pl.BlockSpec(memory_space=pltpu.VMEM)
        hb = pl.BlockSpec(memory_space=pl.ANY)
        dma = pltpu.SemaphoreType.DMA
        return pl.pallas_call(
            functools.partial(kernel, S, TP, H),
            out_shape=jax.ShapeDtypeStruct((T, D), BF16),
            in_specs=[vm] * 7 + [hb] * 5,
            out_specs=hb,
            scratch_shapes=[
                pltpu.VMEM((S, T, hw), BF16),
                pltpu.VMEM((S, T, hw), BF16),
                pltpu.VMEM((S,) + lgt.shape, F32),
                pltpu.VMEM((H, T, hw // H), F32),
                pltpu.VMEM((H, T, hw // H), F32),
                pltpu.VMEM(ow.shape, BF16),
                pltpu.VMEM(gw.shape, BF16),
                pltpu.VMEM(uw.shape, BF16),
                pltpu.VMEM(dw.shape, BF16),
                pltpu.VMEM((R, D), BF16),
                pltpu.VMEM((TP, R, D), BF16),
                pltpu.VMEM((TP, R, D), BF16),
                pltpu.VMEM((R, D), F32),
                pltpu.VMEM((S, R, C), BF16),
                pltpu.VMEM((TP, S, R, C), BF16),
                pltpu.VMEM((2, T, U), F32),
                pltpu.VMEM((S, 2, T, U), BF16),
                pltpu.VMEM((S + 1, 2, T, U), BF16),
                pltpu.VMEM((S, T, U), BF16),
                pltpu.VMEM((TP, S, R, C), BF16),
                pltpu.VMEM((TP, S, R, C), BF16),
                pltpu.VMEM((S, R, C), BF16),
                pltpu.VMEM((S, R, C), BF16),
                pltpu.VMEM((TP, R, D), BF16),
                dma((5,)),
                dma((S, 3)),
                dma((S, 3)),
                dma((TP,)),
                dma((TP,)),
                dma((S,)),
                dma((S,)),
                dma((TP, S)),
                dma((TP, S)),
                dma((S, 2)),
                dma((S + 1, 2)),
                dma((S,)),
                dma((S,)),
                dma((S,)),
                dma((TP, S)),
                dma((TP, S)),
                dma((S,)),
                dma((S,)),
                dma((TP,)),
                dma((TP,)),
                dma((TP,)),
            ],
            compiler_params=pltpu.CompilerParams(
                collective_id=0, has_side_effects=True, vmem_limit_bytes=67043328 - 2**20
            ),
        )(q, k, v, lgt, mg[None], fg[None], og[None], res, ow, gw, uw, dw)

    placed = (
        P(("grp", "sp"), "tp"),
        P(("grp", "sp"), "tp"),
        P(("grp", "sp"), "tp"),
        P(("grp", "sp"), "tp"),
        P(("grp", "sp"), None),
        P("tp", None),
        P(),
        P(),
        P(),
        P("sp", "tp"),
        P("sp", "tp"),
        P("sp", "tp"),
    )
    return jax.shard_map(
        shards, mesh=mesh, in_specs=placed, out_specs=P(("grp", "sp"), None), check_vma=False
    )
```

time: 409 us -> 121 us (0.30)
  waiting for transfers between devices: 329 us -> 0 us
  Pallas kernels: 0 us -> 117 us
  blocking collectives: 31.8 us -> 0 us
  between operations: 15.2 us -> 0.01 us
  matrix products: 14 us -> 0 us
  other arithmetic: 10.2 us -> 1.25 us
    all_gather x3 -> x0, waiting for transfers between devices: 257 us -> none  [the longest x1 97.7 us: shards(): lax.all_gather(down_weight, 'sp', axis=0, tiled=True)]
    pallas_call x0 -> x1, Pallas kernels: none -> 117 us  [shards(): pl.pallas_call(functools.partial(kernel, S, TP, H), out_shape=jax.ShapeDt...]
    psum x2 -> x0, waiting for transfers between devices: 70.5 us -> none  [the longest x1 39.8 us: shards(): mixed_rows = lax.psum(head_part.astype(jnp.bfloat16), 'tp')]
    all_gather x3 -> x0, blocking collectives: 31.8 us -> none  [the longest x1 12.4 us: shards(): key_part = lax.all_gather(key_rows, 'sp', axis=0, tiled=True)]
    dot_general x6 -> x0, matrix products: 14 us -> none  [the longest x1 7.24 us: shards(): lax.dot_general(hidden, lax.all_gather(down_weight, 'sp', axis=0, tiled=T...]
    reduce_sum x4 -> x0, other arithmetic: 4.67 us -> none  [the longest x3 3.91 us: normalize(): jnp.mean(payload_table * payload_table, axis=-1, keepdims=True) + epsilon]
  transfers between devices with their start and end apart: 5 -> 0, of which waited for: 5 -> 0; matrix products, arithmetic and copies ran while one was open for 1% -> 0% of each run, Pallas kernels for 0% -> 0%
where the time goes in v1:
time: 121 us
  Pallas kernels  117 us (97%)
  local copies, waits for them, and re-layouts  1.88 us (2%)
  other arithmetic  1.25 us (1%)
    pallas_call x1, Pallas kernels, shards(): pl.pallas_call(functools.partial(kernel, S, TP, H), out_shape=jax.ShapeDt...  117 us

profile of v1, /device:TPU:1, one launch (start us, length us, event | category | flops | bytes accessed | tf_op | source)
XLA Modules:
  0.0 120.6 jit_solution(493417958558045395)
XLA Ops:
  0.0 1.2 %pad_convert_fusion.lg = f32[8,128]{1,0:T(8,128)} fusion(bf16[2,128]{1,0:T(2,128)(2,1)} %bitcast.7), kind=kLoop, calls=%fused_computation | loop fusion | flops 1024 | bytes 4608 | tf_op jit(solution)/shard_map/jit(_pad)/pad | solution.py:396
  1.3 117.5 %shard_map.118 = bf16[128,2048]{1,0:T(8,128)(2,1)} custom-call(bf16[128,256]{1,0:T(8,128)(2,1)} %q.1, bf16[128,256]{1,0:T(8,128)(2,1)} %k.1, bf16[128,256]{1,0:T(8,128)(2,1)} %v.1, f32[8,128]{1,0:T(8,128)} %pad_convert_fusion.lg, f32[1,2048]{1,0:T(1,128)} %bitcast.4, f32[1,2048]{1,0:T(1,128)} %bitcast.5, f32[1,2048]{1,0:T(1,128)} %bitcast.6, ...), custom_call_target="tpu_custom_call" | custom-call | tf_op jit(solution)/shard_map/pallas_call | solution.py:400
  118.7 1.9 %copy.14 = bf16[128,2048]{1,0:T(8,128)(2,1)} copy(bf16[128,2048]{1,0:T(8,128)(2,1)} %shard_map.118) | data formatting | bytes 1048576

commit v2 on v1

--- a/solution.py
+++ b/solution.py
@@ -46,11 +46,11 @@
 
 
 def kernel(
-    S, TP, H,
+    S, TP, H, pieces,
     q, k, v, lg, mg, fg, og, res, ow, gw, uw, dw,
     out,
     kb, vb, lb, acc, run, owv, gwv, uwv, dwv, resv,
-    hs, hr, mid, ns, na, tmp, gs, gr, hall, us, ur, zs, zr, oall,
+    hs, hr, mid, zs_sum, ns, na, tmp, gs, gr, hall, us, ur, zs, zr, oall,
     loc, kvs, kvr, hss, hrs, n1s, n1r, n2s, n2r, gss, grs, hars, hals, har,
     upss, upr, zss, zrs, oss, ors, outs,
 ):
@@ -191,96 +191,136 @@
     def arrive(s):
         others(TP, tp, lambda t: remote(na.at[tp, s], na.at[t, s], n2s.at[t, s], n2r.at[t, s], "tp", t).wait_recv())
 
-    def partial(j):
-        arrive(j)
+    W = gs.shape[-1]
+
+    def partial(p, j):
+        @pl.when(p == 0)
+        def _():
+            arrive(j)
+
         x = na[:, j].reshape(T, C)
-        tmp[0] = jnp.dot(x, gwv[...], preferred_element_type=F32)
-        tmp[1] = jnp.dot(x, uwv[...], preferred_element_type=F32)
-
-    def g_copy(j, slot, i, peer):
-        return remote(gs.at[j, i], gr.at[slot, i], gss.at[j, i], grs.at[slot, i], "sp", peer)
-
-    def chain(j, first, slot, peer):
-        partial(j)
+        units = pl.ds(pl.multiple_of(p * W, W), W)
+        tmp[0] = jnp.dot(x, gwv[:, units], preferred_element_type=F32)
+        tmp[1] = jnp.dot(x, uwv[:, units], preferred_element_type=F32)
+
+    def g_copy(p, j, slot, peer):
+        return remote(gs.at[p, j], gr.at[p, slot], gss.at[p, j], grs.at[p, slot], "sp", peer)
+
+    def chain(p, j, first, slot, peer):
+        partial(p, j)
 
         @pl.when(first)
         def _():
-            for i in range(2):
-                gs[j, i] = tmp[i].astype(BF16)
-                g_copy(j, slot, i, peer).start()
+            gs[p, j] = tmp[...].astype(BF16)
 
         @pl.when(jnp.logical_not(first))
         def _():
-            for i in range(2):
-                g_copy(j, j, i, peer).wait_recv()
-                gs[j, i] = (tmp[i] + gr[j, i].astype(F32)).astype(BF16)
-                g_copy(j, slot, i, peer).start()
-
-    def reduce_step(tau, carry):
+            g_copy(p, j, j, peer).wait_recv()
+            gs[p, j] = (tmp[...] + gr[p, j].astype(F32)).astype(BF16)
+
+        g_copy(p, j, slot, peer).start()
+
+    def h_right(p, b):
+        return remote(hall.at[p, b], hall.at[p, b], hars.at[p, b], har.at[p, b], "sp", right)
+
+    def h_left(p, b):
+        return remote(hall.at[p, b], hall.at[p, b], hals.at[p, b], har.at[p, b], "sp", left)
+
+    def reduce_step(p, tau):
         jr = S - 1 - tau + me
         jl = tau - (S - 1 - me)
 
         @pl.when((jr > me) & (jr < S))
         def _():
-            chain(jr, me == 0, jr, right)
+            chain(p, jr, me == 0, jr, right)
 
         @pl.when((jl >= 0) & (jl < me))
         def _():
-            chain(jl, me == S - 1, lax.select(jl == me - 1, S, jl), left)
+            chain(p, jl, me == S - 1, lax.select(jl == me - 1, S, jl), left)
+
+    def finish(p):
+        partial(p, me)
+
+        @pl.when(me > 0)
+        def _():
+            g_copy(p, me, me, left).wait_recv()
+            tmp[...] += gr[p, me].astype(F32)
+
+        @pl.when(me < S - 1)
+        def _():
+            g_copy(p, me, S, right).wait_recv()
+            tmp[...] += gr[p, S].astype(F32)
+
+        gate = tmp[0]
+        hall[p, me] = (gate / (1.0 + jnp.exp(-gate)) * tmp[1]).astype(BF16)
+
+        @pl.when(me < S - 1)
+        def _():
+            h_right(p, me).start()
+
+        @pl.when(me > 0)
+        def _():
+            h_left(p, me).start()
+
+    def spread(p, i, then):
+        lo, hi = me - 1 - i, me + 1 + i
+
+        @pl.when(lo >= 0)
+        def _():
+            h_right(p, lo).wait_recv()
+
+            @pl.when(me < S - 1)
+            def _():
+                h_right(p, lo).start()
+
+            then(lo)
+
+        @pl.when(hi < S)
+        def _():
+            h_left(p, hi).wait_recv()
+
+            @pl.when(me > 0)
+            def _():
+                h_left(p, hi).start()
+
+            then(hi)
+
+    def step(g, carry):
+        p, tau = g // (S - 1), lax.rem(g, S - 1)
+
+        @pl.when(p < pieces)
+        def _():
+            reduce_step(p, tau)
+
+        @pl.when((tau == 0) & (p >= 1))
+        def _():
+            finish(p - 1)
+
+        @pl.when(p >= 2)
+        def _():
+            spread(p - 2, tau, lambda b: None)
 
         return carry
 
-    lax.fori_loop(0, S - 1, reduce_step, 0)
-    partial(me)
-    for i in range(2):
-
-        @pl.when(me > 0)
-        def _():
-            g_copy(me, me, i, left).wait_recv()
-            tmp[i] += gr[me, i].astype(F32)
-
-        @pl.when(me < S - 1)
-        def _():
-            g_copy(me, S, i, right).wait_recv()
-            tmp[i] += gr[S, i].astype(F32)
-
-    gate = tmp[0]
-    hall[me] = (gate / (1.0 + jnp.exp(-gate)) * tmp[1]).astype(BF16)
-
-    def h_right(b):
-        return remote(hall.at[b], hall.at[b], hars.at[b], har.at[b], "sp", right)
-
-    def h_left(b):
-        return remote(hall.at[b], hall.at[b], hals.at[b], har.at[b], "sp", left)
-
-    @pl.when(me < S - 1)
-    def _():
-        h_right(me).start()
-
-    @pl.when(me > 0)
-    def _():
-        h_left(me).start()
+    lax.fori_loop(0, (pieces + 1) * (S - 1), step, 0)
 
     def up_copy(t, slot, b):
         return remote(us.at[t, b], ur.at[slot, b], upss.at[t, b], upr.at[slot, b], "tp", t)
 
     def down(b):
-        us[:, b] = nt(hall[b], dwv[...]).astype(BF16).reshape(TP, R, C)
+        rows_b = jnp.concatenate([hall[p, b] for p in range(pieces)], axis=1)
+        us[:, b] = nt(rows_b, dwv[...]).astype(BF16).reshape(TP, R, C)
         others(TP, tp, lambda t: up_copy(t, tp, b).start())
 
     def z_copy(b, slot):
         return remote(zs.at[b], zr.at[slot], zss.at[b], zrs.at[slot], "sp", b)
 
     def settle(b):
-        total = us[tp, b].astype(F32)
-        mid2 = [total]
-
         def add(t):
             up_copy(t, t, b).wait_recv()
             zs_sum[...] += ur[t, b].astype(F32)
 
-        zs_sum = tmp.at[0, pl.ds(0, R), pl.ds(0, C)]
-        zs_sum[...] = mid2[0]
+        zs_sum[...] = us[tp, b].astype(F32)
         others(TP, tp, add)
         zs[b] = zs_sum[...].astype(BF16)
 
@@ -291,32 +331,11 @@
     loads[4].wait()
     down(me)
 
-    def spread(i, carry):
-        lo, hi = me - 1 - i, me + 1 + i
-
-        @pl.when(lo >= 0)
-        def _():
-            h_right(lo).wait_recv()
-
-            @pl.when(me < S - 1)
-            def _():
-                h_right(lo).start()
-
-            down(lo)
-
-        @pl.when(hi < S)
-        def _():
-            h_left(hi).wait_recv()
-
-            @pl.when(me > 0)
-            def _():
-                h_left(hi).start()
-
-            down(hi)
-
+    def last(i, carry):
+        spread(pieces - 1, i, down)
         return carry
 
-    lax.fori_loop(0, S - 1, spread, 0)
+    lax.fori_loop(0, S - 1, last, 0)
     others(S, me, settle)
     settle(me)
     zr[me] = zs[me]
@@ -349,7 +368,7 @@
             def _():
                 for c in kv_copies(b, False):
                     c.wait_send()
-                h_right(b).wait_send()
+                each(pieces, lambda p: h_right(p, b).wait_send())
 
         each(S, sent)
 
@@ -358,15 +377,14 @@
         def sent(b):
             @pl.when(b >= me)
             def _():
-                h_left(b).wait_send()
+                each(pieces, lambda p: h_left(p, b).wait_send())
 
         each(S, sent)
 
     def sp_sent(j):
         n1_copy(j, me).wait_send()
         z_copy(j, me).wait_send()
-        for i in range(2):
-            g_copy(j, j, i, right).wait_send()
+        each(pieces, lambda p: g_copy(p, j, j, right).wait_send())
 
     others(S, me, sp_sent)
 
@@ -392,13 +410,15 @@
         D = res.shape[1]
         C, U = gw.shape
         R = T // TP
+        pieces = max([p for p in range(1, 6) if U % (128 * p) == 0], default=1)
+        W = U // pieces
         pad = -H % 8
         lgt = jnp.pad(lg.astype(F32).T, ((0, pad), (0, 0)))
         vm = pl.BlockSpec(memory_space=pltpu.VMEM)
         hb = pl.BlockSpec(memory_space=pl.ANY)
         dma = pltpu.SemaphoreType.DMA
         return pl.pallas_call(
-            functools.partial(kernel, S, TP, H),
+            functools.partial(kernel, S, TP, H, pieces),
             out_shape=jax.ShapeDtypeStruct((T, D), BF16),
             in_specs=[vm] * 7 + [hb] * 5,
             out_specs=hb,
@@ -416,12 +436,13 @@
                 pltpu.VMEM((TP, R, D), BF16),
                 pltpu.VMEM((TP, R, D), BF16),
                 pltpu.VMEM((R, D), F32),
+                pltpu.VMEM((R, C), F32),
                 pltpu.VMEM((S, R, C), BF16),
                 pltpu.VMEM((TP, S, R, C), BF16),
-                pltpu.VMEM((2, T, U), F32),
-                pltpu.VMEM((S, 2, T, U), BF16),
-                pltpu.VMEM((S + 1, 2, T, U), BF16),
-                pltpu.VMEM((S, T, U), BF16),
+                pltpu.VMEM((2, T, W), F32),
+                pltpu.VMEM((pieces, S, 2, T, W), BF16),
+                pltpu.VMEM((pieces, S + 1, 2, T, W), BF16),
+                pltpu.VMEM((pieces, S, T, W), BF16),
                 pltpu.VMEM((TP, S, R, C), BF16),
                 pltpu.VMEM((TP, S, R, C), BF16),
                 pltpu.VMEM((S, R, C), BF16),
@@ -436,11 +457,11 @@
                 dma((S,)),
                 dma((TP, S)),
                 dma((TP, S)),
-                dma((S, 2)),
-                dma((S + 1, 2)),
-                dma((S,)),
-                dma((S,)),
-                dma((S,)),
+                dma((pieces, S)),
+                dma((pieces, S + 1)),
+                dma((pieces, S)),
+                dma((pieces, S)),
+                dma((pieces, S)),
                 dma((TP, S)),
                 dma((TP, S)),
                 dma((S,)),

time: 121 us -> 123 us (1.017)
  Pallas kernels: 117 us -> 119 us
    pallas_call x1, Pallas kernels: 117 us -> 119 us  [shards(): pl.pallas_call(functools.partial(kernel, S, TP, H, pieces), out_shape=jax...]
where the time goes in v2:
time: 123 us
  Pallas kernels  119 us (97%)
  local copies, waits for them, and re-layouts  1.88 us (2%)
  other arithmetic  1.25 us (1%)
    pallas_call x1, Pallas kernels, shards(): pl.pallas_call(functools.partial(kernel, S, TP, H, pieces), out_shape=jax...  119 us

profile of v2, /device:TPU:1, one launch (start us, length us, event | category | flops | bytes accessed | tf_op | source)
XLA Modules:
  0.0 122.5 jit_solution(4274475585568357795)
XLA Ops:
  0.0 1.2 %pad_convert_fusion.lg = f32[8,128]{1,0:T(8,128)} fusion(bf16[2,128]{1,0:T(2,128)(2,1)} %bitcast.7), kind=kLoop, calls=%fused_computation | loop fusion | flops 1024 | bytes 4608 | tf_op jit(solution)/shard_map/jit(_pad)/pad | solution.py:416
  1.3 119.4 %shard_map.118 = bf16[128,2048]{1,0:T(8,128)(2,1)} custom-call(bf16[128,256]{1,0:T(8,128)(2,1)} %q.1, bf16[128,256]{1,0:T(8,128)(2,1)} %k.1, bf16[128,256]{1,0:T(8,128)(2,1)} %v.1, f32[8,128]{1,0:T(8,128)} %pad_convert_fusion.lg, f32[1,2048]{1,0:T(1,128)} %bitcast.4, f32[1,2048]{1,0:T(1,128)} %bitcast.5, f32[1,2048]{1,0:T(1,128)} %bitcast.6, ...), custom_call_target="tpu_custom_call" | custom-call | tf_op jit(solution)/shard_map/pallas_call | solution.py:420
  120.6 1.9 %copy.14 = bf16[128,2048]{1,0:T(8,128)(2,1)} copy(bf16[128,2048]{1,0:T(8,128)(2,1)} %shard_map.118) | data formatting | bytes 1048576

commit v3 on v2

--- a/solution.py
+++ b/solution.py
@@ -11,6 +11,8 @@
 MESH = pl.DeviceIdType.MESH
 F32 = jnp.float32
 BF16 = jnp.bfloat16
+LAG = 2
+MOST_PIECES = 5
 
 
 def normalize(rows):
@@ -192,6 +194,7 @@
         others(TP, tp, lambda t: remote(na.at[tp, s], na.at[t, s], n2s.at[t, s], n2r.at[t, s], "tp", t).wait_recv())
 
     W = gs.shape[-1]
+    lag = LAG
 
     def partial(p, j):
         @pl.when(p == 0)
@@ -226,17 +229,28 @@
     def h_left(p, b):
         return remote(hall.at[p, b], hall.at[p, b], hals.at[p, b], har.at[p, b], "sp", left)
 
-    def reduce_step(p, tau):
-        jr = S - 1 - tau + me
-        jl = tau - (S - 1 - me)
-
-        @pl.when((jr > me) & (jr < S))
-        def _():
-            chain(p, jr, me == 0, jr, right)
-
-        @pl.when((jl >= 0) & (jl < me))
-        def _():
-            chain(p, jl, me == S - 1, lax.select(jl == me - 1, S, jl), left)
+    def cut(at):
+        return lax.div(at, S - 1), lax.rem(at, S - 1)
+
+    def reduce_step(g):
+        at_right = g - me * lag
+        at_left = g - (S - 1 - me) * lag
+
+        @pl.when((at_right >= 0) & (at_right < pieces * (S - 1)))
+        def _():
+            p, tau = cut(at_right)
+
+            @pl.when(S - 1 - tau > me)
+            def _():
+                chain(p, S - 1 - tau, me == 0, S - 1 - tau, right)
+
+        @pl.when((at_left >= 0) & (at_left < pieces * (S - 1)))
+        def _():
+            p, j = cut(at_left)
+
+            @pl.when(j < me)
+            def _():
+                chain(p, j, me == S - 1, lax.select(j == me - 1, S, j), left)
 
     def finish(p):
         partial(p, me)
@@ -286,23 +300,28 @@
             then(hi)
 
     def step(g, carry):
-        p, tau = g // (S - 1), lax.rem(g, S - 1)
-
-        @pl.when(p < pieces)
-        def _():
-            reduce_step(p, tau)
-
-        @pl.when((tau == 0) & (p >= 1))
-        def _():
-            finish(p - 1)
-
-        @pl.when(p >= 2)
-        def _():
-            spread(p - 2, tau, lambda b: None)
-
-        return carry
-
-    lax.fori_loop(0, (pieces + 1) * (S - 1), step, 0)
+        reduce_step(g)
+        at = g - (S - 1) * lag
+        p, tau = cut(at)
+
+        @pl.when((at >= 0) & (tau == 0) & (p < pieces))
+        def _():
+            finish(p)
+
+        def gather(i, carry):
+            at_i = at - (i + 1) * lag
+            p, tau = cut(at_i)
+
+            @pl.when((at_i >= 0) & (tau == 0) & (p < pieces - 1))
+            def _():
+                spread(p, i, lambda b: None)
+
+            return carry
+
+        return lax.fori_loop(0, S - 1, gather, carry)
+
+    steps = (S - 1) * (lag + max(pieces - 1, pieces - 2 + lag)) + 1
+    lax.fori_loop(0, steps, step, 0)
 
     def up_copy(t, slot, b):
         return remote(us.at[t, b], ur.at[slot, b], upss.at[t, b], upr.at[slot, b], "tp", t)
@@ -410,7 +429,7 @@
         D = res.shape[1]
         C, U = gw.shape
         R = T // TP
-        pieces = max([p for p in range(1, 6) if U % (128 * p) == 0], default=1)
+        pieces = max([p for p in range(1, MOST_PIECES + 1) if U % (128 * p) == 0], default=1)
         W = U // pieces
         pad = -H % 8
         lgt = jnp.pad(lg.astype(F32).T, ((0, pad), (0, 0)))

time: 123 us -> 115 us (0.935)
  Pallas kernels: 119 us -> 111 us
    pallas_call x1, Pallas kernels: 119 us -> 111 us  [shards(): pl.pallas_call(functools.partial(kernel, S, TP, H, pieces), out_shape=jax...]
where the time goes in v3:
time: 115 us; the launch traced here: 114 us
  Pallas kernels  111 us (97%)
  local copies, waits for them, and re-layouts  1.88 us (2%)
  other arithmetic  1.25 us (1%)
    pallas_call x1, Pallas kernels, shards(): pl.pallas_call(functools.partial(kernel, S, TP, H, pieces), out_shape=jax...  111 us

profile of v3, /device:TPU:1, one launch (start us, length us, event | category | flops | bytes accessed | tf_op | source)
XLA Modules:
  0.0 114.4 jit_solution(5704049129599492754)
XLA Ops:
  0.0 1.2 %pad_convert_fusion.lg = f32[8,128]{1,0:T(8,128)} fusion(bf16[2,128]{1,0:T(2,128)(2,1)} %bitcast.7), kind=kLoop, calls=%fused_computation | loop fusion | flops 1024 | bytes 4608 | tf_op jit(solution)/shard_map/jit(_pad)/pad | solution.py:435
  1.3 111.3 %shard_map.118 = bf16[128,2048]{1,0:T(8,128)(2,1)} custom-call(bf16[128,256]{1,0:T(8,128)(2,1)} %q.1, bf16[128,256]{1,0:T(8,128)(2,1)} %k.1, bf16[128,256]{1,0:T(8,128)(2,1)} %v.1, f32[8,128]{1,0:T(8,128)} %pad_convert_fusion.lg, f32[1,2048]{1,0:T(1,128)} %bitcast.4, f32[1,2048]{1,0:T(1,128)} %bitcast.5, f32[1,2048]{1,0:T(1,128)} %bitcast.6, ...), custom_call_target="tpu_custom_call" | custom-call | tf_op jit(solution)/shard_map/pallas_call | solution.py:439
  112.6 1.9 %copy.14 = bf16[128,2048]{1,0:T(8,128)(2,1)} copy(bf16[128,2048]{1,0:T(8,128)(2,1)} %shard_map.118) | data formatting | bytes 1048576
